TPU v7x, 1024 devices: a whole 4x8x16 slice. The times are simulated.
1024 devices in a mesh: ep: 32 (over z, core), tp: 32 (over y, x).
Axes of the slice: x: 4, y: 8, z: 16, core: 2. Of those that a mesh axis runs over, the one named last changes fastest.
Arguments:
- tokens: bfloat16 [512, 4096], P('ep', 'tp'), may hold values from -40 to 40
- routes: int32 [512, 4], P('ep'), may hold values from 0 to 63, all different within a row; in each aligned block of 16 rows (0 to 15, 16 to 31, ...) at most 2 rows name the same one
- gates: float32 [512, 4], P('ep'), may hold values from 0.1 to 1
- pre_gain: bfloat16 [4096], P('tp'), may hold values from 0.099609375 to 1.8984375
- expert_gate: bfloat16 [64, 4096, 1024], P('ep', 'tp'), may hold values from -0.09375 to 0.09375
- expert_up: bfloat16 [64, 4096, 1024], P('ep', 'tp'), may hold values from -0.09375 to 0.09375
- expert_down: bfloat16 [64, 1024, 4096], P('ep', None, 'tp'), may hold values from -0.125 to 0.125
- shared_gate: bfloat16 [4096, 1024], P('tp'), may hold values from -0.09375 to 0.09375
- shared_up: bfloat16 [4096, 1024], P('tp'), may hold values from -0.09375 to 0.09375
- shared_down: bfloat16 [1024, 4096], P(None, 'tp'), may hold values from -0.125 to 0.125
- out_gain: bfloat16 [4096], P('tp'), may hold values from 0.099609375 to 1.8984375
Outputs:
- mixed: bfloat16 [512, 4096], P('ep', 'tp')
Inputs may be any that keep to these rules, and one draw needn't show every extreme that they name: `routes`: each row names 4 different experts, and expert e is held by index e // 2 of ep. Among the 16 rows of one index of ep no expert is named by more than 2 rows, and in every draw some expert is named by exactly 2 rows of some index.
All inputs are finite; a program needn't handle non-finite values.
Results may differ from a plain program's by a relative error of at most 0.012.
Values may be sent and summed in bfloat16 or wider, within the bound.
A program may use at most 32 MiB of HBM per device.

v0:
```python
import jax
import jax.numpy as jnp
from jax import lax
from jax.sharding import PartitionSpec as P

D = 4096


def in_blocks(shard, dim, peers):
    before, after = (shard.shape[:dim], shard.shape[dim + 1 :])
    return jnp.moveaxis(shard.reshape(*before, peers, -1, *after), dim, 0)


def sent_and_summed(shard, axis, dim):
    peers = lax.axis_size(axis)
    tiles = lax.all_to_all(in_blocks(shard, dim, peers), axis, 0, 0, tiled=True)
    return jnp.sum(tiles.astype(jnp.float32), axis=0)


def side_by_side(arrays, axis, dim, along):
    widths = [a.shape[along] for a in arrays]
    both = jnp.concatenate(arrays, axis=along)
    filled = sent_and_summed(both, axis, dim)
    return tuple(jnp.split(filled, [sum(widths[:k]) for k in range(1, len(widths))], axis=along))


def rows_first(arrays, axis, dims):
    turned = [jnp.moveaxis(a, dim, 0) for a, dim in zip(arrays, dims)]
    both = jnp.concatenate([t.reshape(len(t), -1) for t in turned], axis=1)
    filled, at, outs = (lax.all_gather(both, axis, axis=0, tiled=True), 0, [])
    for t, dim in zip(turned, dims):
        section = filled[:, at : at + t[0].size].reshape(-1, *t.shape[1:])
        outs.append(jnp.moveaxis(section, 0, dim))
        at += t[0].size
    return tuple(outs)


def sent_to_all(shard, axis):
    peers = lax.axis_size(axis)
    return lax.all_to_all(
        jnp.broadcast_to(shard[None], (peers, *shard.shape)), axis, 0, 0, tiled=True
    )


def over_copies(shard, axis):
    return sent_to_all(shard, axis).sum(axis=0)


def normalize(values, gain, squares, width):
    scale = lax.rsqrt(squares[:, None] / width + 1e-06)
    return values * scale * gain.astype(jnp.float32)


def expert_apply(buffer, expert_gate, expert_up, expert_down, shared_gate_part, shared_up_part):
    gate_part = jnp.einsum(
        "secd,edf->secf", buffer, expert_gate, preferred_element_type=jnp.float32
    )
    up_part = jnp.einsum("secd,edf->secf", buffer, expert_up, preferred_element_type=jnp.float32)
    full_shape = gate_part.shape
    row_count = full_shape[0] * full_shape[1] * full_shape[2]
    gate_rows = gate_part.reshape(row_count, full_shape[3])
    up_rows = up_part.reshape(row_count, full_shape[3])
    gate_share, up_share, shared_gate_share, shared_up_share = side_by_side(
        (
            gate_rows.astype(jnp.bfloat16),
            up_rows.astype(jnp.bfloat16),
            shared_gate_part.astype(jnp.bfloat16),
            shared_up_part.astype(jnp.bfloat16),
        ),
        "tp",
        1,
        0,
    )
    hidden_share = (jax.nn.silu(gate_share) * up_share).astype(jnp.bfloat16)
    shared_share = (jax.nn.silu(shared_gate_share) * shared_up_share).astype(jnp.bfloat16)
    hidden_rows, shared_hidden = rows_first((hidden_share, shared_share), "tp", (1, 1))
    hidden = hidden_rows.reshape(full_shape)
    results = jnp.einsum(
        "secf,efd->secd", hidden, expert_down, preferred_element_type=jnp.float32
    ).astype(jnp.bfloat16)
    return (results, shared_hidden)


def on_device(
    tokens,
    routes,
    gates,
    pre_gain,
    expert_gate,
    expert_up,
    expert_down,
    shared_gate,
    shared_up,
    shared_down,
    out_gain,
):
    own_rows = tokens.astype(jnp.float32)
    in_squares = over_copies(jnp.sum(own_rows * own_rows, axis=1), "tp")
    normed = normalize(own_rows, pre_gain, in_squares, D).astype(jnp.bfloat16)
    shared_gate_part = jnp.dot(normed, shared_gate, preferred_element_type=jnp.float32)
    shared_up_part = jnp.dot(normed, shared_up, preferred_element_type=jnp.float32)
    tok_count = tokens.shape[0]
    top_count = routes.shape[1]
    groups = lax.axis_size("ep")
    local_experts = expert_gate.shape[0]
    experts_all = local_experts * groups
    capacity = max(2, 3 * tok_count * top_count // (2 * experts_all))
    places = jnp.arange(capacity, dtype=jnp.int32)
    zero_value = jnp.zeros((), jnp.float32)
    labels = jnp.arange(experts_all, dtype=jnp.int32)
    picked = routes[:, :, None] == labels[None, None, :]
    onehot = jnp.sum(picked.astype(jnp.int32), axis=1)
    dense_gate = jnp.sum(jnp.where(picked, gates[:, :, None], zero_value), axis=1)
    slot_index = jnp.cumsum(onehot, axis=0) - onehot
    select = (slot_index.T[:, None, :] == places[None, :, None]) & (onehot.T[:, None, :] > 0)
    outgoing = jnp.einsum(
        "ect,td->ecd", select.astype(jnp.bfloat16), normed, preferred_element_type=jnp.float32
    ).astype(jnp.bfloat16)
    outgoing = outgoing.reshape(groups, local_experts, capacity, normed.shape[1])
    received = lax.all_to_all(outgoing, "ep", split_axis=0, concat_axis=0, tiled=True)
    results, shared_hidden = expert_apply(
        received, expert_gate, expert_up, expert_down, shared_gate_part, shared_up_part
    )
    returned = lax.all_to_all(results, "ep", split_axis=0, concat_axis=0, tiled=True)
    weight = jnp.where(select, dense_gate.T[:, None, :], zero_value)
    returned_rows = returned.reshape(experts_all, capacity, normed.shape[1]).astype(jnp.float32)
    routed = jnp.einsum("ect,ecd->td", weight, returned_rows, precision=lax.Precision.HIGHEST)
    shared_out = jnp.dot(shared_hidden, shared_down, preferred_element_type=jnp.float32)
    combined = routed + shared_out
    out_squares = over_copies(jnp.sum(combined * combined, axis=1), "tp")
    return normalize(combined, out_gain, out_squares, D).astype(jnp.bfloat16)


def solution(mesh):
    in_specs = (
        P("ep", "tp"),
        P("ep", None),
        P("ep", None),
        P("tp"),
        P("ep", "tp", None),
        P("ep", "tp", None),
        P("ep", None, "tp"),
        P("tp", None),
        P("tp", None),
        P(None, "tp"),
        P("tp"),
    )
    out_specs = P("ep", "tp")
    return jax.shard_map(
        on_device, mesh=mesh, in_specs=in_specs, out_specs=out_specs, check_vma=False
    )
```

profile of v0, /device:TPU:1, one launch (start us, length us, event | category | flops | bytes accessed | tf_op | source)
XLA Modules:
  0.0 167.3 jit_solution(2424527635686730110)
XLA Ops:
  0.0 0.9 fusion.18
  0.9 0.6 broadcast_in_dim.32
  1.5 10.5 %all-to-all-start = ((f32[32,1,16]{2,1,0:T(1,128)}), f32[32,1,16]{2,1,0:T(1,128)S(1)}, u32[]{:S(2)}, u32[]{:S(2)}) async-start(f32[32,1,16]{2,1,0:T(1,128)} %broadcast_in_dim.32), calls=%async_computation | async-start | bytes 32768 | tf_op jit(solution)/shard_map/all_to_all | solution.py:40
  12.0 0.8 convert_reduce_fusion.1
  12.8 0.7 convert_element_type.64
  13.4 7.2 %all-to-all-done = f32[32,1,16]{2,1,0:T(1,128)S(1)} async-done(((f32[32,1,16]{2,1,0:T(1,128)}), f32[32,1,16]{2,1,0:T(1,128)S(1)}, u32[]{:S(2)}, u32[]{:S(2)}) %all-to-all-start) | async-done | bytes 2080 | tf_op jit(solution)/shard_map/all_to_all | solution.py:40
  20.7 0.9 convolution_convert_fusion.5
  21.6 0.6 copy.46
  22.2 20.9 %all-to-all-start.1 = ((bf16[32,2,2,128]{3,2,1,0:T(2,128)(2,1)}), bf16[32,2,2,128]{3,2,1,0:T(2,128)(2,1)S(1)}, u32[]{:S(2)}, u32[]{:S(2)}) async-start(bf16[32,2,2,128]{3,2,1,0:T(2,128)(2,1)} %copy.46), calls=%async_computation.1 | async-start | bytes 65536 | tf_op jit(solution)/shard_map/all_to_all | solution.py:120
  43.1 1.2 convolution_convert_fusion.3
  44.2 1.2 convolution_convert_fusion.4
  45.4 9.7 %all-to-all-done.1 = bf16[32,2,2,128]{3,2,1,0:T(2,128)(2,1)S(1)} async-done(((bf16[32,2,2,128]{3,2,1,0:T(2,128)(2,1)}), bf16[32,2,2,128]{3,2,1,0:T(2,128)(2,1)S(1)}, u32[]{:S(2)}, u32[]{:S(2)}) %all-to-all-start.1) | async-done | bytes 32800 | tf_op jit(solution)/shard_map/all_to_all | solution.py:120
  56.4 1.2 copy.51
  57.6 4.0 %all-to-all-start.2 = ((bf16[32,288,32]{1,2,0:T(8,128)(2,1)}), bf16[32,288,32]{1,2,0:T(8,128)(2,1)S(1)}, u32[]{:S(2)}, u32[]{:S(2)}) async-start(bf16[32,288,32]{1,2,0:T(8,128)(2,1)} %bitcast.12), calls=%async_computation.2 | async-start | bytes 1572864 | tf_op jit(solution)/shard_map/all_to_all | solution.py:16
  61.7 20.9 %all-to-all-done.2 = bf16[32,288,32]{1,2,0:T(8,128)(2,1)S(1)} async-done(((bf16[32,288,32]{1,2,0:T(8,128)(2,1)}), bf16[32,288,32]{1,2,0:T(8,128)(2,1)S(1)}, u32[]{:S(2)}, u32[]{:S(2)}) %all-to-all-start.2) | async-done | bytes 589856 | tf_op jit(solution)/shard_map/all_to_all | solution.py:16
  82.8 37.6 %all_gather.3 = bf16[1024,144]{1,0:T(8,128)(2,1)S(1)} all-gather(bf16[32,144]{1,0:T(8,128)(2,1)S(1)} %pad_maximum_fusion.1), channel_id=1, replica_groups=mesh['ep'=32,'tp'=32] {'tp'}, dimensions={0}, use_global_device_ids=true | all-gather | bytes 304128 | tf_op jit(solution)/shard_map/all_gather | solution.py:30
  120.8 0.7 copy-done.2
  121.8 0.6 copy.54
  122.4 17.5 %all-to-all-start.3 = ((bf16[32,2,2,128]{3,2,1,0:T(2,128)(2,1)}), bf16[32,2,2,128]{3,2,1,0:T(2,128)(2,1)S(1)}, u32[]{:S(2)}, u32[]{:S(2)}) async-start(bf16[32,2,2,128]{3,2,1,0:T(2,128)(2,1)} %copy.54), calls=%async_computation.3 | async-start | bytes 65536 | tf_op jit(solution)/shard_map/all_to_all | solution.py:124
  140.1 12.0 %all-to-all-done.3 = bf16[32,2,2,128]{3,2,1,0:T(2,128)(2,1)S(1)} async-done(((bf16[32,2,2,128]{3,2,1,0:T(2,128)(2,1)}), bf16[32,2,2,128]{3,2,1,0:T(2,128)(2,1)S(1)}, u32[]{:S(2)}, u32[]{:S(2)}) %all-to-all-start.3) | async-done | bytes 32800 | tf_op jit(solution)/shard_map/all_to_all | solution.py:124
  152.5 0.6 broadcast_in_dim.33
  153.1 4.8 %all-to-all-start.4 = ((f32[32,1,16]{2,1,0:T(1,128)}), f32[32,1,16]{2,1,0:T(1,128)S(1)}, u32[]{:S(2)}, u32[]{:S(2)}) async-start(f32[32,1,16]{2,1,0:T(1,128)} %broadcast_in_dim.33), calls=%async_computation.4 | async-start | bytes 32768 | tf_op jit(solution)/shard_map/all_to_all | solution.py:40
  157.9 8.6 %all-to-all-done.4 = f32[32,1,16]{2,1,0:T(1,128)S(1)} async-done(((f32[32,1,16]{2,1,0:T(1,128)}), f32[32,1,16]{2,1,0:T(1,128)S(1)}, u32[]{:S(2)}, u32[]{:S(2)}) %all-to-all-start.4) | async-done | bytes 2080 | tf_op jit(solution)/shard_map/all_to_all | solution.py:40
  166.6 0.7 multiply_convert_fusion
  (40 shorter events, 2.8 us)
Async XLA Ops:
  0.0 55.1 %copy-start = (bf16[2,128,1024]{2,1,0:T(8,128)(2,1)S(1)}, bf16[2,128,1024]{2,1,0:T(8,128)(2,1)}, u32[]{:S(2)}) copy-start(bf16[2,128,1024]{2,1,0:T(8,128)(2,1)} %param.15) | copy-start | bytes 1572868
  1.5 19.1 %all-to-all-start = ((f32[32,1,16]{2,1,0:T(1,128)}), f32[32,1,16]{2,1,0:T(1,128)S(1)}, u32[]{:S(2)}, u32[]{:S(2)}) async-start(f32[32,1,16]{2,1,0:T(1,128)} %broadcast_in_dim.32), calls=%async_computation | async-start | bytes 32768 | tf_op jit(solution)/shard_map/all_to_all | solution.py:40
  22.2 32.9 %all-to-all-start.1 = ((bf16[32,2,2,128]{3,2,1,0:T(2,128)(2,1)}), bf16[32,2,2,128]{3,2,1,0:T(2,128)(2,1)S(1)}, u32[]{:S(2)}, u32[]{:S(2)}) async-start(bf16[32,2,2,128]{3,2,1,0:T(2,128)(2,1)} %copy.46), calls=%async_computation.1 | async-start | bytes 65536 | tf_op jit(solution)/shard_map/all_to_all | solution.py:120
  45.4 10.3 %copy-start.1 = (bf16[2,128,1024]{2,1,0:T(8,128)(2,1)S(1)}, bf16[2,128,1024]{2,1,0:T(8,128)(2,1)}, u32[]{:S(2)}) copy-start(bf16[2,128,1024]{2,1,0:T(8,128)(2,1)} %param.16) | copy-start | bytes 1572868
  57.6 4.1 %copy-start.4 = (s32[16,4]{0,1:T(4,128)S(1)}, s32[16,4]{0,1:T(4,128)}, u32[]{:S(2)}) copy-start(s32[16,4]{0,1:T(4,128)} %param.12) | copy-start | bytes 772
  57.6 4.1 %copy-start.5 = (f32[16,4]{0,1:T(4,128)S(1)}, f32[16,4]{0,1:T(4,128)}, u32[]{:S(2)}) copy-start(f32[16,4]{0,1:T(4,128)} %param.13) | copy-start | bytes 772
  57.6 25.1 %all-to-all-start.2 = ((bf16[32,288,32]{1,2,0:T(8,128)(2,1)}), bf16[32,288,32]{1,2,0:T(8,128)(2,1)S(1)}, u32[]{:S(2)}, u32[]{:S(2)}) async-start(bf16[32,288,32]{1,2,0:T(8,128)(2,1)} %bitcast.12), calls=%async_computation.2 | async-start | bytes 1572864 | tf_op jit(solution)/shard_map/all_to_all | solution.py:16
  120.5 1.0 copy-start.2
  120.7 19.2 %copy-start.3 = (bf16[1024,128]{1,0:T(8,128)(2,1)S(1)}, bf16[1024,128]{1,0:T(8,128)(2,1)}, u32[]{:S(2)}) copy-start(bf16[1024,128]{1,0:T(8,128)(2,1)} %param.20) | copy-start | bytes 786436
  121.5 36.4 %copy-start.6 = (bf16[128]{0:T(256)(128)(2,1)S(1)}, bf16[128]{0:T(256)(128)(2,1)}, u32[]{:S(2)}) copy-start(bf16[128]{0:T(256)(128)(2,1)} %param.21) | copy-start | bytes 772
  122.4 29.7 %all-to-all-start.3 = ((bf16[32,2,2,128]{3,2,1,0:T(2,128)(2,1)}), bf16[32,2,2,128]{3,2,1,0:T(2,128)(2,1)S(1)}, u32[]{:S(2)}, u32[]{:S(2)}) async-start(bf16[32,2,2,128]{3,2,1,0:T(2,128)(2,1)} %copy.54), calls=%async_computation.3 | async-start | bytes 65536 | tf_op jit(solution)/shard_map/all_to_all | solution.py:124
  153.1 13.4 %all-to-all-start.4 = ((f32[32,1,16]{2,1,0:T(1,128)}), f32[32,1,16]{2,1,0:T(1,128)S(1)}, u32[]{:S(2)}, u32[]{:S(2)}) async-start(f32[32,1,16]{2,1,0:T(1,128)} %broadcast_in_dim.33), calls=%async_computation.4 | async-start | bytes 32768 | tf_op jit(solution)/shard_map/all_to_all | solution.py:40
where the time goes:
time: 168 us; the launch traced here: 167 us
  waiting for transfers between devices  58.4 us (35%)
  starting transfers between devices  57.7 us (34%)
  blocking collectives  37.6 us (22%)
  local copies, waits for them, and re-layouts  5.44 us (3%)
  matrix products  4.43 us (3%)
  other arithmetic  3.47 us (2%)
    all_gather x1, blocking collectives, rows_first(): filled, at, outs = (lax.all_gather(both, axis, axis=0, tiled=True), 0, [])  37.6 us
    all_to_all x1, waiting for transfers between devices, sent_and_summed(): tiles = lax.all_to_all(in_blocks(shard, dim, peers), axis, 0, 0, tiled=True)  20.9 us
    all_to_all x1, starting transfers between devices, on_device(): lax.all_to_all(outgoing, 'ep', split_axis=0, concat_axis=0, tiled=True)  20.9 us
    all_to_all x1, starting transfers between devices, on_device(): lax.all_to_all(results, 'ep', split_axis=0, concat_axis=0, tiled=True)  17.5 us
    all_to_all x2, waiting for transfers between devices, sent_to_all(): lax.all_to_all(jnp.broadcast_to(shard[None], (peers, *shard.shape)), axis...  15.8 us
    all_to_all x2, starting transfers between devices, sent_to_all(): lax.all_to_all(jnp.broadcast_to(shard[None], (peers, *shard.shape)), axis...  15.3 us
    all_to_all x1, waiting for transfers between devices, on_device(): lax.all_to_all(results, 'ep', split_axis=0, concat_axis=0, tiled=True)  12 us
    all_to_all x1, waiting for transfers between devices, on_device(): lax.all_to_all(outgoing, 'ep', split_axis=0, concat_axis=0, tiled=True)  9.71 us
  transfers between devices with their start and end apart: 5, of which 5 were waited for; matrix products, arithmetic and copies ran while one was open for 2% of the time, Pallas kernels for 0%

commit v1 on v0

v1 whole, which is shorter than its diff:
```python
import jax
import jax.numpy as jnp
from jax import lax
from jax.experimental import pallas as pl
from jax.experimental.pallas import tpu as pltpu
from jax.sharding import PartitionSpec as P

MESH = pl.DeviceIdType.MESH
BF = jnp.bfloat16
F32 = jnp.float32
D = 4096.0
EPS = 1e-06
NX, NY, NZ = 4, 8, 16
NEP, NTP = 32, 32
DYS = (4, 3, 5, 2, 6, 1, 7, 0)
NT = (((1,), (1,)), ((), ()))
NN = (((1,), (0,)), ((), ()))


def dot(a, b, dims=NN):
    return lax.dot_general(a, b, dims, preferred_element_type=F32)


def ep_target(i, z, c):
    j = i // 2
    k = (j + 1) // 2
    dz = jnp.where(j % 2 == 0, 8 + k, 8 - k)
    core = (c + 1 + i) % 2
    return ((z + dz) % NZ) * 2 + core


def tp_target(i, y, x):
    j = i // 4
    k = (j + 1) // 2
    dy = jnp.where(j % 2 == 0, 4 + k, 4 - k)
    dx = 2 + i % 4
    dx = jnp.where(i % 4 == 1, 1, jnp.where(i % 4 == 2, 3, jnp.where(i % 4 == 3, 0, 2)))
    return ((y + dy) % NY) * NX + (x + dx) % NX


def kernel(
    tok_h, routes_h, gates_h, pg_h, eg_h, eu_h, ed_h, sg_h, su_h, sd_h, og_h,
    out_ref,
    tok, routes, gates, pg, eg, eu, ed, sg, su, sd, og,
    wt, swt, dt, asend, arecv, rows, tail, xbd, sxbd,
    xsend, xrecv, ysend, yrecv, hid, hsh, dsend, drecv, esend, erecv,
    in_sem, a_s, a_r, bx_s, bx_r, by_s, by_r, c_s, c_r, cs_s, cs_r, d_s, d_r, e_s, e_r,
):
    me_ep, me_tp = lax.axis_index("ep"), lax.axis_index("tp")
    z, c = me_ep // 2, me_ep % 2
    y, x = me_tp // NX, me_tp % NX

    barrier = pltpu.get_barrier_semaphore()

    def greet(i, carry):
        pl.semaphore_signal(barrier, inc=1, device_id=(ep_target(i, z, c), me_tp), device_id_type=MESH)
        pl.semaphore_signal(barrier, inc=1, device_id=(me_ep, tp_target(i, y, x)), device_id_type=MESH)
        return carry

    lax.fori_loop(0, 31, greet, 0)

    pairs = (
        (tok_h, tok), (routes_h, routes), (gates_h, gates), (pg_h, pg), (og_h, og),
        (eg_h, eg), (eu_h, eu), (sg_h, sg), (su_h, su), (ed_h, ed), (sd_h, sd),
    )
    loads = [pltpu.make_async_copy(a, b, in_sem.at[k]) for k, (a, b) in enumerate(pairs)]
    for load in loads:
        load.start()
    for load in loads[:5]:
        load.wait()

    lane = lax.broadcasted_iota(jnp.int32, (16, 128), 1)
    sub = lax.broadcasted_iota(jnp.int32, (16, 128), 0)
    named = jnp.zeros((16, 128), F32)
    weight = jnp.zeros((16, 128), F32)
    for k in range(4):
        hit = routes[:, k : k + 1] == lane // 2
        named = named + jnp.where(hit, 1.0, 0.0)
        weight = weight + jnp.where(hit, gates[:, k : k + 1], 0.0)
    low = jnp.where(
        lax.broadcasted_iota(jnp.int32, (16, 16), 1) < lax.broadcasted_iota(jnp.int32, (16, 16), 0), 1.0, 0.0
    )
    slot = dot(low.astype(BF), named.astype(BF))
    chosen = (named > 0.5) & (jnp.abs(slot - (lane % 2).astype(F32)) < 0.5)
    select = jnp.where(chosen, 1.0, 0.0)
    weight = jnp.where(chosen, weight, 0.0)
    own = tok[...]
    rows[...] = dot(select.T.astype(BF), own)
    for b in range(NEP):
        asend[b] = rows[4 * b : 4 * b + 4, :].astype(BF)

    for load in loads[5:7]:
        load.wait()
    for k in range(8):
        for half, source in enumerate((eg, eu)):
            for e in range(2):
                wt[k, 128 * half : 128 * half + 128, 128 * e : 128 * e + 128] = source[
                    e, :, 128 * k : 128 * k + 128
                ].T

    pl.semaphore_wait(barrier, 62)

    def dispatch(i, carry):
        to = ep_target(i, z, c)
        pltpu.make_async_remote_copy(
            src_ref=asend.at[to], dst_ref=arecv.at[me_ep], send_sem=a_s, recv_sem=a_r,
            device_id=(to, me_tp), device_id_type=MESH,
        ).start()
        return carry

    lax.fori_loop(0, 31, dispatch, 0)
    arecv[me_ep] = asend[me_ep]

    for load in loads[7:]:
        load.wait()
    for k in range(8):
        for half, source in enumerate((sg, su)):
            swt[128 * half : 128 * half + 128, 128 * k : 128 * k + 128] = source[:, 128 * k : 128 * k + 128].T
        for e in range(2):
            dt[128 * e : 128 * e + 128, 128 * k : 128 * k + 128] = ed[e, 128 * k : 128 * k + 128, :].T
    gain = pg[...].astype(F32)
    own32 = own.astype(F32)
    sxbd[...] = jnp.zeros_like(sxbd)
    own_gained = (own32 * gain).astype(BF)
    for g in range(8):
        sxbd[16 * g : 16 * g + 16, 128 * g : 128 * g + 128] = own_gained
    rows2 = dot(swt[...], sxbd[...], NT)
    own_squares = jnp.sum(own32 * own32, axis=1, keepdims=True)
    own_line = jnp.sum(jnp.where(lane % 16 == sub, own_squares, 0.0), axis=0, keepdims=True)
    own_line_hi = own_line.astype(BF).astype(F32)
    tail[...] = jnp.zeros_like(tail)
    for p in range(NTP):
        tail[p, 0:4, :] = rows2[4 * p : 4 * p + 4, :]
        tail[p, 4:8, :] = rows2[128 + 4 * p : 132 + 4 * p, :]

    pltpu.make_async_copy(arecv.at[pl.ds(0, 31)], arecv.at[pl.ds(0, 31)], a_r).wait()
    for b in range(NEP):
        rows[4 * b : 4 * b + 4, :] = arecv[b].astype(F32)
    came = rows[...]
    r0 = lax.broadcasted_iota(jnp.int32, (128, 128), 0)
    r1 = lax.broadcasted_iota(jnp.int32, (128, 128), 1)
    squares = jnp.sum(came * came, axis=1, keepdims=True)
    line = jnp.sum(jnp.where(r0 == r1, squares, 0.0), axis=0, keepdims=True)
    line_hi = line.astype(BF).astype(F32)
    came_gained = came * gain
    first = (r0 // 2) % 2 == 0
    xbd[:, 0:128] = jnp.where(first, came_gained, 0.0).astype(BF)
    xbd[:, 128:256] = jnp.where(first, 0.0, came_gained).astype(BF)
    sums = jnp.where(sub == 8, line_hi, 0.0) + jnp.where(sub == 9, line - line_hi, 0.0)
    sums = sums + jnp.where(sub == 10, own_line_hi, 0.0) + jnp.where(sub == 11, own_line - own_line_hi, 0.0)

    for dy in DYS:
        yp = (y + dy) % NY
        part = dot(wt[yp], xbd[...], NT)
        for xp in range(NX):
            xsend[yp, xp, 0:32, :] = part[32 * xp : 32 * xp + 32, :].astype(BF)
            xsend[yp, xp, 32:64, :] = part[128 + 32 * xp : 160 + 32 * xp, :].astype(BF)
            xsend[yp, xp, 64:80, :] = (tail[yp * NX + xp] + sums).astype(BF)
        for dx in (2, 1, 3):
            xp = (x + dx) % NX
            pltpu.make_async_remote_copy(
                src_ref=xsend.at[yp, xp], dst_ref=xrecv.at[yp, x], send_sem=bx_s, recv_sem=bx_r.at[yp, x],
                device_id=(me_ep, y * NX + xp), device_id_type=MESH,
            ).start()

    total = None
    for dy in DYS:
        yp = (y + dy) % NY
        acc = xsend[yp, x].astype(F32)
        for dx in (1, 3, 2):
            xp = (x + dx) % NX
            pltpu.make_async_remote_copy(
                src_ref=xsend.at[yp, xp], dst_ref=xrecv.at[yp, xp], send_sem=bx_s, recv_sem=bx_r.at[yp, xp],
                device_id=(me_ep, y * NX + xp), device_id_type=MESH,
            ).wait_recv()
            acc = acc + xrecv[yp, xp].astype(F32)
        if dy == 0:
            total = acc
        else:
            end = acc[64:80, :]
            lost = end - end.astype(BF).astype(F32)
            lost = jnp.where((sub == 9) | (sub == 11), pltpu.roll(lost, 1, 0), 0.0)
            ysend[yp, 0:64, :] = acc[0:64, :].astype(BF)
            ysend[yp, 64:80, :] = (end + lost).astype(BF)
            pltpu.make_async_remote_copy(
                src_ref=ysend.at[yp], dst_ref=yrecv.at[y], send_sem=by_s, recv_sem=by_r.at[y],
                device_id=(me_ep, yp * NX + x), device_id_type=MESH,
            ).start()

    for dy in (1, 7, 2, 6, 3, 5, 4):
        yp = (y + dy) % NY
        pltpu.make_async_remote_copy(
            src_ref=ysend.at[yp], dst_ref=yrecv.at[yp], send_sem=by_s, recv_sem=by_r.at[yp],
            device_id=(me_ep, yp * NX + x), device_id_type=MESH,
        ).wait_recv()
        total = total + yrecv[yp].astype(F32)

    scale = lax.rsqrt((total[72:73, :] + total[73:74, :]) / D + EPS)
    own_scale = lax.rsqrt((total[74:75, :] + total[75:76, :]) / D + EPS)
    gate_v = total[0:32, :] * scale
    hid[me_tp] = (gate_v / (1.0 + jnp.exp(-gate_v)) * (total[32:64, :] * scale)).astype(BF)
    gate_s = total[64:68, :] * own_scale
    hsh[me_tp] = (gate_s / (1.0 + jnp.exp(-gate_s)) * (total[68:72, :] * own_scale)).astype(BF)

    def hidden_copies(p, to, sem_slot):
        return (
            pltpu.make_async_remote_copy(
                src_ref=hid.at[p], dst_ref=hid.at[p], send_sem=c_s, recv_sem=c_r.at[sem_slot],
                device_id=(me_ep, to), device_id_type=MESH,
            ),
            pltpu.make_async_remote_copy(
                src_ref=hsh.at[p], dst_ref=hsh.at[p], send_sem=cs_s, recv_sem=cs_r.at[sem_slot],
                device_id=(me_ep, to), device_id_type=MESH,
            ),
        )

    for dy in DYS[:-1]:
        for copy in hidden_copies(me_tp, ((y + dy) % NY) * NX + x, me_tp):
            copy.start()
    for dy in (0, 1, 7, 2, 6, 3, 5, 4):
        p = ((y + dy) % NY) * NX + x
        if dy != 0:
            for copy in hidden_copies(p, p, p):
                copy.wait_recv()
        for dx in (2, 1, 3):
            for copy in hidden_copies(p, y * NX + (x + dx) % NX, p):
                copy.start()
    for dy in (0, 1, 7, 2, 6, 3, 5, 4):
        for dx in (1, 3, 2):
            p = ((y + dy) % NY) * NX + (x + dx) % NX
            for copy in hidden_copies(p, y * NX + (x + dx) % NX, p):
                copy.wait_recv()

    both = dot(dt[...], hid[...].reshape(1024, 128))
    back = jnp.where((r1 // 2) % 2 == 0, both[0:128, :], both[128:256, :])
    rows[...] = back.T
    for b in range(NEP):
        dsend[b] = rows[4 * b : 4 * b + 4, :].astype(BF)

    def give_back(i, carry):
        to = ep_target(i, z, c)
        pltpu.make_async_remote_copy(
            src_ref=dsend.at[to], dst_ref=drecv.at[me_ep], send_sem=d_s, recv_sem=d_r,
            device_id=(to, me_tp), device_id_type=MESH,
        ).start()
        return carry

    lax.fori_loop(0, 31, give_back, 0)
    drecv[me_ep] = dsend[me_ep]

    for p in range(NTP):
        rows[4 * p : 4 * p + 4, :] = hsh[p].astype(F32)
    turned = rows[...].T
    shared_out = jnp.zeros((16, 128), F32)
    for g in range(8):
        shared_out = shared_out + dot(turned[16 * g : 16 * g + 16, :].astype(BF), sd[128 * g : 128 * g + 128, :])
    w_hi = weight.astype(BF)
    rest = weight - w_hi.astype(F32)
    w_mid = rest.astype(BF)
    w_lo = (rest - w_mid.astype(F32)).astype(BF)

    pltpu.make_async_copy(drecv.at[pl.ds(0, 31)], drecv.at[pl.ds(0, 31)], d_r).wait()
    for b in range(NEP):
        rows[4 * b : 4 * b + 4, :] = drecv[b].astype(F32)
    given = rows[...].astype(BF)
    combined = dot(w_hi, given) + dot(w_mid, given) + dot(w_lo, given) + shared_out

    out_squares = jnp.sum(combined * combined, axis=1, keepdims=True)
    out_line = jnp.sum(jnp.where(lane == sub, out_squares, 0.0), axis=0, keepdims=True)
    esend[...] = out_line

    def tell(i, carry):
        to = tp_target(i, y, x)
        pltpu.make_async_remote_copy(
            src_ref=esend, dst_ref=erecv.at[me_tp], send_sem=e_s, recv_sem=e_r,
            device_id=(me_ep, to), device_id_type=MESH,
        ).start()
        return carry

    lax.fori_loop(0, 31, tell, 0)
    erecv[me_tp] = out_line
    pltpu.make_async_copy(erecv.at[pl.ds(0, 31)], erecv.at[pl.ds(0, 31)], e_r).wait()
    all_squares = jnp.sum(erecv[...], axis=0)
    column = jnp.sum(jnp.where(lane == sub, all_squares, 0.0), axis=1, keepdims=True)
    out_scale = lax.rsqrt(column / D + EPS)
    out_ref[...] = (combined * out_scale * og[...].astype(F32)).astype(BF)

    for ref, sem in (
        (asend.at[pl.ds(0, 31)], a_s), (xsend.at[pl.ds(0, 6)], bx_s), (ysend.at[pl.ds(0, 7)], by_s),
        (hid.at[pl.ds(0, 31)], c_s), (hsh.at[pl.ds(0, 31)], cs_s), (dsend.at[pl.ds(0, 31)], d_s),
        (erecv.at[pl.ds(0, 31)], e_s),
    ):
        pltpu.make_async_copy(ref, ref, sem).wait()


def solution(mesh):
    def on_device(tokens, routes, gates, pre_gain, eg, eu, ed, sg, su, sd, out_gain):
        dma = pltpu.SemaphoreType.DMA
        return pl.pallas_call(
            kernel,
            name="experts",
            out_shape=jax.ShapeDtypeStruct((16, 128), BF),
            in_specs=[pl.BlockSpec(memory_space=pl.ANY)] * 11,
            out_specs=pl.BlockSpec(memory_space=pltpu.VMEM),
            scratch_shapes=[
                pltpu.VMEM((16, 128), BF), pltpu.VMEM((16, 4), jnp.int32), pltpu.VMEM((16, 4), F32),
                pltpu.VMEM((1, 128), BF), pltpu.VMEM((2, 128, 1024), BF), pltpu.VMEM((2, 128, 1024), BF),
                pltpu.VMEM((2, 1024, 128), BF), pltpu.VMEM((128, 1024), BF), pltpu.VMEM((128, 1024), BF),
                pltpu.VMEM((1024, 128), BF), pltpu.VMEM((1, 128), BF),
                pltpu.VMEM((8, 256, 256), BF), pltpu.VMEM((256, 1024), BF), pltpu.VMEM((256, 1024), BF),
                pltpu.VMEM((32, 4, 128), BF), pltpu.VMEM((32, 4, 128), BF), pltpu.VMEM((128, 128), F32),
                pltpu.VMEM((32, 16, 128), F32), pltpu.VMEM((128, 256), BF), pltpu.VMEM((128, 1024), BF),
                pltpu.VMEM((8, 4, 80, 128), BF), pltpu.VMEM((8, 4, 80, 128), BF),
                pltpu.VMEM((8, 80, 128), BF), pltpu.VMEM((8, 80, 128), BF),
                pltpu.VMEM((32, 32, 128), BF), pltpu.VMEM((32, 4, 128), BF),
                pltpu.VMEM((32, 4, 128), BF), pltpu.VMEM((32, 4, 128), BF),
                pltpu.VMEM((1, 128), F32), pltpu.VMEM((32, 1, 128), F32),
                dma((11,)), dma, dma, dma, dma((8, 4)), dma, dma((8,)), dma, dma((32,)), dma, dma((32,)),
                dma, dma, dma, dma,
            ],
            compiler_params=pltpu.CompilerParams(collective_id=0, has_side_effects=True),
        )(tokens, routes, gates, pre_gain.reshape(1, 128), eg, eu, ed, sg, su, sd, out_gain.reshape(1, 128))

    return jax.shard_map(
        on_device,
        mesh=mesh,
        in_specs=(
            P("ep", "tp"), P("ep", None), P("ep", None), P("tp"), P("ep", "tp", None), P("ep", "tp", None),
            P("ep", None, "tp"), P("tp", None), P("tp", None), P(None, "tp"), P("tp"),
        ),
        out_specs=P("ep", "tp"),
        check_vma=False,
    )
```

time: 168 us -> 69.8 us (0.42)
  Pallas kernels: 0 us -> 66.2 us
  waiting for transfers between devices: 58.4 us -> 0 us
  starting transfers between devices: 57.7 us -> 0 us
  blocking collectives: 37.6 us -> 0 us
  matrix products: 4.43 us -> 0 us
  other arithmetic: 3.47 us -> 0 us
  local copies, waits for them, and re-layouts: 5.44 us -> 3.31 us
    pallas_call x0 -> x1, Pallas kernels: none -> 66.2 us  [on_device(): pl.pallas_call(kernel, name='experts', out_shape=jax.ShapeDtypeStruct((16...]
    all_to_all x5 -> x0, waiting for transfers between devices: 58.4 us -> none  [the longest x1 20.9 us: sent_and_summed(): tiles = lax.all_to_all(in_blocks(shard, dim, peers), axis, 0, 0, tiled=True)]
    all_to_all x5 -> x0, starting transfers between devices: 57.7 us -> none  [the longest x1 20.9 us: on_device(): lax.all_to_all(outgoing, 'ep', split_axis=0, concat_axis=0, tiled=True)]
    all_gather x1 -> x0, blocking collectives: 37.6 us -> none  [rows_first(): filled, at, outs = (lax.all_gather(both, axis, axis=0, tiled=True), 0, [])]
    dot_general x8 -> x0, matrix products: 4.43 us -> none  [the longest x1 1.17 us: on_device(): jnp.dot(normed, shared_gate, preferred_element_type=jnp.float32)]
    unnamed x14 -> x7, local copies, waits for them, and re-layouts: 0.77 us -> 3.31 us
    reduce_sum x6 -> x0, other arithmetic: 1.93 us -> none  [the longest x1 0.86 us: on_device(): in_squares = over_copies(jnp.sum(own_rows * own_rows, axis=1), 'tp')]
  transfers between devices with their start and end apart: 5 -> 0, of which waited for: 5 -> 0; matrix products, arithmetic and copies ran while one was open for 2% -> 0% of each run, Pallas kernels for 0% -> 0%
where the time goes in v1:
time: 69.8 us; the launch traced here: 69.6 us
  Pallas kernels  66.2 us (95%)
  local copies, waits for them, and re-layouts  3.31 us (5%)
    pallas_call x1, Pallas kernels, on_device(): pl.pallas_call(kernel, name='experts', out_shape=jax.ShapeDtypeStruct((16...  66.2 us
    unnamed x7, local copies, waits for them, and re-layouts  3.31 us

profile of v1, /device:TPU:1, one launch (start us, length us, event | category | flops | bytes accessed | tf_op | source)
XLA Modules:
  0.0 69.6 jit_solution(5400316811663347441)
XLA Ops:
  0.0 0.0 copy-start
  0.0 0.7 copy-done
  0.7 0.0 copy-start.1
  0.7 0.7 copy.12.routes_h
  1.4 0.0 copy-done.1
  1.4 0.7 copy.13.gates_h
  2.0 66.2 %experts.1 = bf16[16,128]{1,0:T(8,128)(2,1)} custom-call(bf16[16,128]{1,0:T(8,128)(2,1)} %tok_h.1, s32[16,4]{1,0:T(8,128)} %copy.12.routes_h, f32[16,4]{1,0:T(8,128)} %copy.13.gates_h, bf16[1,128]{1,0:T(2,128)(2,1)} %bitcast.2, bf16[2,128,1024]{2,1,0:T(8,128)(2,1)} %eg_h.1, bf16[2,128,1024]{2,1,0:T(8,128)(2,1)} %eu_h.1, bf16[2,1024,128]{2,1,0:T(8,128)(2,1)} %ed_h.1, ...), custom_call_target="tpu_custom_call" | custom-call | tf_op jit(solution)/shard_map/experts/pallas_call | solution.py:299
  68.3 1.3 %copy.15 = bf16[16,128]{1,0:T(8,128)(2,1)} copy(bf16[16,128]{1,0:T(8,128)(2,1)} %experts.1) | data formatting | bytes 8192
Async XLA Ops:
  0.0 0.7 copy-start
  0.7 0.7 copy-start.1

commit v2 on v1

v2 whole, which is shorter than its diff:
```python
import jax
import jax.numpy as jnp
from jax import lax
from jax.experimental import pallas as pl
from jax.experimental.pallas import tpu as pltpu
from jax.sharding import PartitionSpec as P

MESH = pl.DeviceIdType.MESH
BF = jnp.bfloat16
F32 = jnp.float32
D = 4096.0
EPS = 1e-06
NX, NY, NZ = 4, 8, 16
NEP, NTP = 32, 32
FAR_Z = (8, 7, 9, 6, 10, 5, 11, 4, 12, 3, 13, 2, 14, 1, 15, 0)
FAR_Y = (4, 3, 5, 2, 6, 1, 7, 0)
NEAR_Y = (0, 1, 7, 2, 6, 3, 5, 4)
FAR_X = (2, 1, 3, 0)
NT = (((1,), (1,)), ((), ()))
NN = (((1,), (0,)), ((), ()))


def dot(a, b, dims=NN):
    return lax.dot_general(a, b, dims, preferred_element_type=F32)


def silu(v):
    return v / (1.0 + jnp.exp(-v))


def kernel(
    tok_h, routes_h, gates_h, pg_h, eg_h, eu_h, ed_h, sg_h, su_h, sd_h, og_h,
    out_ref,
    tok, routes, gates, pg, eg, eu, ed, sg, su, sd, og,
    wt, swt, dt, asend, arecv, rows, xbd, sxbd,
    ssend, srecv, hsh, xsend, xrecv, ysend, yrecv, qsend, qrecv, hid, dsend, drecv, esend, erecv,
    in_sem, a_s, a_r, s_s, s_r, h_s, h_r, bx_s, bx_r, by_s, by_r, q_s, q_r, c_s, c_r, d_s, d_r, e_s, e_r,
):
    me_ep, me_tp = lax.axis_index("ep"), lax.axis_index("tp")
    z, c = me_ep // 2, me_ep % 2
    y, x = me_tp // NX, me_tp % NX
    zs = {d: (z + d) % NZ for d in FAR_Z}
    ys = {d: (y + d) % NY for d in FAR_Y}
    xs = {d: (x + d) % NX for d in FAR_X}
    far_ep = [2 * zs[d] + (c if same else 1 - c) for d in FAR_Z for same in (0, 1) if d or not same]
    far_tp = [NX * ys[dy] + xs[dx] for dy in FAR_Y for dx in FAR_X if dy or dx]

    def send(src, dst, send_sem, recv_sem, ep=None, tp=None):
        return pltpu.make_async_remote_copy(
            src_ref=src, dst_ref=dst, send_sem=send_sem, recv_sem=recv_sem,
            device_id=(me_ep if ep is None else ep, me_tp if tp is None else tp), device_id_type=MESH,
        )

    def wait_bytes(ref, sem):
        pltpu.make_async_copy(ref, ref, sem).wait()

    pairs = (
        (tok_h, tok), (routes_h, routes), (gates_h, gates), (pg_h, pg), (og_h, og),
        (eg_h, eg), (eu_h, eu), (sg_h, sg), (su_h, su), (ed_h, ed), (sd_h, sd),
    )
    loads = [pltpu.make_async_copy(a, b, in_sem.at[k]) for k, (a, b) in enumerate(pairs)]
    for load in loads[:3]:
        load.start()
    barrier = pltpu.get_barrier_semaphore()
    for to in far_ep:
        pl.semaphore_signal(barrier, inc=1, device_id=(to, me_tp), device_id_type=MESH)
    for to in far_tp:
        pl.semaphore_signal(barrier, inc=1, device_id=(me_ep, to), device_id_type=MESH)
    for load in loads[3:]:
        load.start()
    for load in loads[:5]:
        load.wait()

    lane = lax.broadcasted_iota(jnp.int32, (16, 128), 1)
    sub = lax.broadcasted_iota(jnp.int32, (16, 128), 0)
    row = lax.broadcasted_iota(jnp.int32, (128, 16), 0)
    named = jnp.zeros((128, 16), F32)
    weight = jnp.zeros((128, 16), F32)
    for k in range(4):
        hit = routes[k : k + 1, :] == row // 2
        named = named + jnp.where(hit, 1.0, 0.0)
        weight = weight + jnp.where(hit, gates[k : k + 1, :], 0.0)
    earlier = jnp.where(
        lax.broadcasted_iota(jnp.int32, (16, 16), 0) < lax.broadcasted_iota(jnp.int32, (16, 16), 1), 1.0, 0.0
    )
    slot = dot(named.astype(BF), earlier.astype(BF))
    chosen = (named > 0.5) & (jnp.abs(slot - (row % 2).astype(F32)) < 0.5)
    select = jnp.where(chosen, 1.0, 0.0)
    weight = jnp.where(chosen, weight, 0.0).T
    w_hi = weight.astype(BF)
    rest = weight - w_hi.astype(F32)
    w_mid = rest.astype(BF)
    w_lo = (rest - w_mid.astype(F32)).astype(BF)
    own = tok[...]
    rows[...] = dot(select.astype(BF), own)
    for b in range(NEP):
        asend[b] = rows[4 * b : 4 * b + 4, :].astype(BF)
    arecv[me_ep] = asend[me_ep]

    for load in loads[5:]:
        load.wait()
    for k in range(8):
        for s, source in enumerate((eg, eu)):
            for e in range(2):
                at = 128 * (2 * s + e)
                wt[k, :, at : at + 128] = source[e, :, 128 * k : 128 * k + 128].T
        for half, source in enumerate((sg, su)):
            swt[128 * half : 128 * half + 128, 128 * k : 128 * k + 128] = source[:, 128 * k : 128 * k + 128].T
    for e in range(2):
        for half in range(2):
            for k in range(4):
                units = [ed[e, 32 * p + 16 * half : 32 * p + 16 * half + 16, :] for p in range(8 * k, 8 * k + 8)]
                at = 128 * (2 * half + e)
                dt[at : at + 128, 128 * k : 128 * k + 128] = jnp.concatenate(units, axis=0).T
    gain = pg[...].astype(F32)
    own32 = own.astype(F32)
    sxbd[...] = jnp.zeros_like(sxbd)
    own_gained = (own32 * gain).astype(BF)
    for g in range(8):
        sxbd[16 * g : 16 * g + 16, 128 * g : 128 * g + 128] = own_gained
    shared_part = dot(swt[...], sxbd[...], NT)
    own_squares = jnp.sum(own32 * own32, axis=1, keepdims=True)
    own_line = jnp.sum(jnp.where(lane % 16 == sub, own_squares, 0.0), axis=0, keepdims=True)
    own_line_hi = own_line.astype(BF).astype(F32)
    own_sums = jnp.where(sub == 8, own_line_hi, 0.0) + jnp.where(sub == 9, own_line - own_line_hi, 0.0)
    for p in range(NTP):
        rows[0:4, :] = shared_part[4 * p : 4 * p + 4, :]
        rows[4:8, :] = shared_part[128 + 4 * p : 132 + 4 * p, :]
        rows[8:16, :] = own_sums[8:16, :]
        ssend[p] = rows[0:16, :].astype(BF)
    srecv[me_tp] = ssend[me_tp]

    pl.semaphore_wait(barrier, 62)
    for to in far_ep:
        send(asend.at[to], arecv.at[me_ep], a_s, a_r.at[z // 8], ep=to).start()
    for to in far_tp:
        send(ssend.at[to], srecv.at[me_tp], s_s, s_r, tp=to).start()

    r0 = lax.broadcasted_iota(jnp.int32, (64, 128), 0)
    r1 = lax.broadcasted_iota(jnp.int32, (64, 128), 1)
    first = (r0 // 2) % 2 == 0

    def rows_came(ch):
        @pl.when(z // 8 == ch)
        def _():
            wait_bytes(arecv.at[pl.ds(0, 15)], a_r.at[ch])

        @pl.when(z // 8 != ch)
        def _():
            wait_bytes(arecv.at[pl.ds(0, 16)], a_r.at[ch])

    def rows_multiplied(ch):
        for b in range(16):
            rows[4 * b : 4 * b + 4, :] = arecv[16 * ch + b].astype(F32)
        came = rows[0:64, :]
        squares = jnp.sum(came * came, axis=1, keepdims=True)
        line = jnp.sum(jnp.where(r1 % 64 == r0, squares, 0.0), axis=0, keepdims=True)
        gained = came * gain
        e0 = jnp.where(first, gained, 0.0).astype(BF)
        e1 = jnp.where(first, 0.0, gained).astype(BF)
        xbd[ch, 0:64, 0:128] = e0
        xbd[ch, 0:64, 128:256] = e1
        xbd[ch, 0:64, 256:512] = jnp.zeros((64, 256), BF)
        xbd[ch, 64:128, 0:256] = jnp.zeros((64, 256), BF)
        xbd[ch, 64:128, 256:384] = e0
        xbd[ch, 64:128, 384:512] = e1
        qsend[ch] = line
        qrecv[ch, me_tp] = line
        for some in (FAR_Y[:4], FAR_Y[4:]):
            for dy in some:
                part = dot(wt[ys[dy]], xbd[ch], NT)
                for xp in range(NX):
                    xsend[ch, ys[dy] * NX + xp] = part[32 * xp : 32 * xp + 32, :].astype(BF)
            for dy in some:
                yp = ys[dy]
                for dx in (2, 1, 3):
                    xp = xs[dx]
                    send(xsend.at[ch, yp * NX + xp], xrecv.at[ch, yp * NX + x], bx_s.at[ch], bx_r.at[ch, FAR_Y.index(dy) // 2], tp=y * NX + xp).start()
        for to in far_tp:
            send(qsend.at[ch], qrecv.at[ch, me_tp], q_s.at[ch], q_r.at[ch], tp=to).start()

    def summed_over_x(ch):
        total = None
        for at, dy in enumerate(FAR_Y):
            yp = ys[dy]
            if at % 2 == 0:
                wait_bytes(xrecv.at[ch, pl.ds(0, 6)], bx_r.at[ch, at // 2])
            acc = xsend[ch, yp * NX + x].astype(F32)
            for dx in (1, 3, 2):
                acc = acc + xrecv[ch, yp * NX + xs[dx]].astype(F32)
            if dy == 0:
                total = acc
            else:
                ysend[ch, yp] = acc.astype(BF)
                send(ysend.at[ch, yp], yrecv.at[ch, y], by_s.at[ch], by_r.at[ch], tp=yp * NX + x).start()
        return total

    def summed_over_y(ch, total):
        wait_bytes(yrecv.at[ch, pl.ds(0, 7)], by_r.at[ch])
        for dy in NEAR_Y[1:]:
            yp = ys[dy]
            total = total + yrecv[ch, yp].astype(F32)
        wait_bytes(qrecv.at[ch, pl.ds(0, 31)], q_r.at[ch])
        scale = lax.rsqrt(jnp.sum(qrecv[ch], axis=0) / D + EPS)
        v = total * scale
        h = silu(v) * pltpu.roll(v, 64, 1)
        hid[ch, me_tp] = jnp.where(lane < 64, h[0:16, :], pltpu.roll(h[16:32, :], 64, 1)).astype(BF)
        for to in far_tp:
            send(hid.at[ch, me_tp], hid.at[ch, me_tp], c_s.at[ch], c_r.at[ch], tp=to).start()

    def gathered(ch):
        wait_bytes(hid.at[ch, pl.ds(0, 31)], c_r.at[ch])

    def given_back(ch):
        both = dot(dt[...], hid[ch].reshape(512, 128))
        even = (lax.broadcasted_iota(jnp.int32, (128, 128), 1) // 2) % 2 == 0
        low = jnp.where(even, both[0:128, :], both[128:256, :])
        high = jnp.where(even, both[256:384, :], both[384:512, :])
        rows[...] = (low + pltpu.roll(high, 64, 1)).T
        for b in range(16):
            dsend[16 * ch + b] = rows[4 * b : 4 * b + 4, :].astype(BF)
        for b in range(16 * ch, 16 * ch + 16):
            @pl.when(me_ep != b)
            def _():
                send(dsend.at[b], drecv.at[me_ep], d_s, d_r, ep=b).start()

    rows_came(0)
    rows_multiplied(0)
    total0 = summed_over_x(0)
    rows_came(1)
    rows_multiplied(1)
    summed_over_y(0, total0)

    wait_bytes(srecv.at[pl.ds(0, 31)], s_r)
    shared_sum = jnp.sum(srecv[...].astype(F32), axis=0)
    own_scale = lax.rsqrt((shared_sum[8:9, :] + shared_sum[9:10, :]) / D + EPS)
    hsh[me_tp] = (silu(shared_sum[0:4, :] * own_scale) * (shared_sum[4:8, :] * own_scale)).astype(BF)
    for to in far_tp:
        send(hsh.at[me_tp], hsh.at[me_tp], h_s, h_r, tp=to).start()

    total1 = summed_over_x(1)
    summed_over_y(1, total1)
    gathered(0)
    given_back(0)
    gathered(1)
    given_back(1)
    drecv[me_ep] = dsend[me_ep]

    wait_bytes(hsh.at[pl.ds(0, 31)], h_r)
    for p in range(NTP):
        rows[4 * p : 4 * p + 4, :] = hsh[p].astype(F32)
    turned = rows[...].T.astype(BF)
    shared_out = jnp.zeros((16, 128), F32)
    for g in range(8):
        shared_out = shared_out + dot(turned[16 * g : 16 * g + 16, :], sd[128 * g : 128 * g + 128, :])

    wait_bytes(drecv.at[pl.ds(0, 31)], d_r)
    for b in range(NEP):
        rows[4 * b : 4 * b + 4, :] = drecv[b].astype(F32)
    given = rows[...].astype(BF)
    combined = dot(w_hi, given) + dot(w_mid, given) + dot(w_lo, given) + shared_out
    out_squares = jnp.sum(combined * combined, axis=1, keepdims=True)
    out_line = jnp.sum(jnp.where(lane == sub, out_squares, 0.0), axis=0, keepdims=True)
    esend[...] = out_line
    for to in far_tp:
        send(esend, erecv.at[me_tp], e_s, e_r, tp=to).start()
    erecv[me_tp] = out_line
    wait_bytes(erecv.at[pl.ds(0, 31)], e_r)
    all_squares = jnp.sum(erecv[...], axis=0)
    column = jnp.sum(jnp.where(lane == sub, all_squares, 0.0), axis=1, keepdims=True)
    out_scale = lax.rsqrt(column / D + EPS)
    out_ref[...] = (combined * out_scale * og[...].astype(F32)).astype(BF)

    for ref, sem in (
        (asend.at[pl.ds(0, 31)], a_s), (ssend.at[pl.ds(0, 31)], s_s), (hsh.at[pl.ds(0, 31)], h_s),
        (dsend.at[pl.ds(0, 31)], d_s), (erecv.at[pl.ds(0, 31)], e_s),
    ):
        wait_bytes(ref, sem)
    for ch in range(2):
        wait_bytes(xsend.at[ch, pl.ds(0, 24)], bx_s.at[ch])
        wait_bytes(ysend.at[ch, pl.ds(0, 7)], by_s.at[ch])
        wait_bytes(hid.at[ch, pl.ds(0, 31)], c_s.at[ch])
        wait_bytes(qrecv.at[ch, pl.ds(0, 31)], q_s.at[ch])


def solution(mesh):
    def on_device(tokens, routes, gates, pre_gain, eg, eu, ed, sg, su, sd, out_gain):
        dma = pltpu.SemaphoreType.DMA
        return pl.pallas_call(
            kernel,
            name="experts",
            out_shape=jax.ShapeDtypeStruct((16, 128), BF),
            in_specs=[pl.BlockSpec(memory_space=pl.ANY)] * 11,
            out_specs=pl.BlockSpec(memory_space=pltpu.VMEM),
            scratch_shapes=[
                pltpu.VMEM((16, 128), BF), pltpu.VMEM((4, 16), jnp.int32), pltpu.VMEM((4, 16), F32),
                pltpu.VMEM((1, 128), BF), pltpu.VMEM((2, 128, 1024), BF), pltpu.VMEM((2, 128, 1024), BF),
                pltpu.VMEM((2, 1024, 128), BF), pltpu.VMEM((128, 1024), BF), pltpu.VMEM((128, 1024), BF),
                pltpu.VMEM((1024, 128), BF), pltpu.VMEM((1, 128), BF),
                pltpu.VMEM((8, 128, 512), BF), pltpu.VMEM((256, 1024), BF), pltpu.VMEM((512, 512), BF),
                pltpu.VMEM((32, 4, 128), BF), pltpu.VMEM((32, 4, 128), BF), pltpu.VMEM((128, 128), F32),
                pltpu.VMEM((2, 128, 512), BF), pltpu.VMEM((128, 1024), BF),
                pltpu.VMEM((32, 16, 128), BF), pltpu.VMEM((32, 16, 128), BF), pltpu.VMEM((32, 4, 128), BF),
                pltpu.VMEM((2, 32, 32, 128), BF), pltpu.VMEM((2, 32, 32, 128), BF),
                pltpu.VMEM((2, 8, 32, 128), BF), pltpu.VMEM((2, 8, 32, 128), BF),
                pltpu.VMEM((2, 1, 128), F32), pltpu.VMEM((2, 32, 1, 128), F32),
                pltpu.VMEM((2, 32, 16, 128), BF),
                pltpu.VMEM((32, 4, 128), BF), pltpu.VMEM((32, 4, 128), BF),
                pltpu.VMEM((1, 128), F32), pltpu.VMEM((32, 1, 128), F32),
                dma((11,)), dma, dma((2,)), dma, dma, dma, dma, dma((2,)), dma((2, 4)), dma((2,)), dma((2,)),
                dma((2,)), dma((2,)), dma((2,)), dma((2,)), dma, dma, dma, dma,
            ],
            compiler_params=pltpu.CompilerParams(collective_id=0, has_side_effects=True),
        )(tokens, routes.T, gates.T, pre_gain.reshape(1, 128), eg, eu, ed, sg, su, sd, out_gain.reshape(1, 128))

    return jax.shard_map(
        on_device,
        mesh=mesh,
        in_specs=(
            P("ep", "tp"), P("ep", None), P("ep", None), P("tp"), P("ep", "tp", None), P("ep", "tp", None),
            P("ep", None, "tp"), P("tp", None), P("tp", None), P(None, "tp"), P("tp"),
        ),
        out_specs=P("ep", "tp"),
        check_vma=False,
    )
```

time: 69.8 us -> 61.9 us (0.89)
  Pallas kernels: 66.2 us -> 60.1 us
  local copies, waits for them, and re-layouts: 3.31 us -> 1.28 us
    pallas_call x1, Pallas kernels: 66.2 us -> 60.1 us  [on_device(): pl.pallas_call(kernel, name='experts', out_shape=jax.ShapeDtypeStruct((16...]
    unnamed x7 -> x1, local copies, waits for them, and re-layouts: 3.31 us -> 1.28 us
where the time goes in v2:
time: 61.9 us; the launch traced here: 61.4 us
  Pallas kernels  60.1 us (97%)
  local copies, waits for them, and re-layouts  1.28 us (2%)
    pallas_call x1, Pallas kernels, on_device(): pl.pallas_call(kernel, name='experts', out_shape=jax.ShapeDtypeStruct((16...  60.1 us
    unnamed x1, local copies, waits for them, and re-layouts  1.28 us

profile of v2, /device:TPU:1, one launch (start us, length us, event | category | flops | bytes accessed | tf_op | source)
XLA Modules:
  0.0 61.4 jit_solution(11712480523662903148)
XLA Ops:
  0.0 60.1 %experts.1 = bf16[16,128]{1,0:T(8,128)(2,1)} custom-call(bf16[16,128]{1,0:T(8,128)(2,1)} %tok_h.1, s32[4,16]{1,0:T(4,128)} %bitcast.4, f32[4,16]{1,0:T(4,128)} %bitcast.5, bf16[1,128]{1,0:T(2,128)(2,1)} %bitcast.6, bf16[2,128,1024]{2,1,0:T(8,128)(2,1)} %eg_h.1, bf16[2,128,1024]{2,1,0:T(8,128)(2,1)} %eu_h.1, bf16[2,1024,128]{2,1,0:T(8,128)(2,1)} %ed_h.1, ...), custom_call_target="tpu_custom_call" | custom-call | tf_op jit(solution)/shard_map/experts/pallas_call | solution.py:289
  60.1 1.3 %copy.13 = bf16[16,128]{1,0:T(8,128)(2,1)} copy(bf16[16,128]{1,0:T(8,128)(2,1)} %experts.1) | data formatting | bytes 8192

commit v3 on v2

v3 whole, which is shorter than its diff:
```python
import jax
import jax.numpy as jnp
from jax import lax
from jax.experimental import pallas as pl
from jax.experimental.pallas import tpu as pltpu
from jax.sharding import PartitionSpec as P

MESH = pl.DeviceIdType.MESH
BF = jnp.bfloat16
F32 = jnp.float32
D = 4096.0
EPS = 1e-06
NX, NY, NZ = 4, 8, 16
NEP, NTP = 32, 32
FAR_Z = (8, 7, 9, 6, 10, 5, 11, 4, 12, 3, 13, 2, 14, 1, 15, 0)
FAR_Y = (4, 3, 5, 2, 6, 1, 7, 0)
NEAR_Y = (0, 1, 7, 2, 6, 3, 5, 4)
FAR_X = (2, 1, 3, 0)
STAGES = ((4, 3, 5), (2, 6, 1, 7, 0))
NT = (((1,), (1,)), ((), ()))
NN = (((1,), (0,)), ((), ()))


def dot(a, b, dims=NN):
    return lax.dot_general(a, b, dims, preferred_element_type=F32)


def silu(v):
    return v / (1.0 + jnp.exp(-v))


def kernel(
    tok_h, routes, gates, pg, eg_h, eu_h, ed_h, sg_h, su_h, sd_h, og,
    out_ref,
    tok, eg, eu, ed, sg, su, sd,
    wt, swt, dt, asend, arecv, rows, xsm, xbd, sxbd,
    ssend, srecv, hsh, bsend, brecv, xsend, xrecv, ysend, yrecv, qsend, qrecv, hid, dsend, drecv, esend, erecv,
    in_sem, a_s, a_r, s_s, s_r, h_s, h_r, b_s, b_r, bx_s, bx_r, by_s, by_r, q_s, q_r, c_s, c_r, d_s, d_r, e_s, e_r,
):
    me_ep, me_tp = lax.axis_index("ep"), lax.axis_index("tp")
    z, c = me_ep // 2, me_ep % 2
    y, x = me_tp // NX, me_tp % NX
    zs = {d: (z + d) % NZ for d in FAR_Z}
    ys = {d: (y + d) % NY for d in FAR_Y}
    xs = {d: (x + d) % NX for d in FAR_X}
    far_ep = [2 * zs[d] + (c if same else 1 - c) for d in FAR_Z for same in (0, 1) if d or not same]
    far_tp = [NX * ys[dy] + xs[dx] for dy in FAR_Y for dx in FAR_X if dy or dx]

    def send(src, dst, send_sem, recv_sem, ep=None, tp=None):
        return pltpu.make_async_remote_copy(
            src_ref=src, dst_ref=dst, send_sem=send_sem, recv_sem=recv_sem,
            device_id=(me_ep if ep is None else ep, me_tp if tp is None else tp), device_id_type=MESH,
        )

    def wait_bytes(ref, sem):
        pltpu.make_async_copy(ref, ref, sem).wait()

    pairs = (
        (tok_h, tok), (eg_h, eg), (eu_h, eu), (sg_h, sg), (su_h, su), (ed_h, ed), (sd_h, sd),
    )
    loads = [pltpu.make_async_copy(a, b, in_sem.at[k]) for k, (a, b) in enumerate(pairs)]
    loads[0].start()
    barrier = pltpu.get_barrier_semaphore()
    for to in far_ep:
        pl.semaphore_signal(barrier, inc=1, device_id=(to, me_tp), device_id_type=MESH)
    for to in far_tp:
        pl.semaphore_signal(barrier, inc=1, device_id=(me_ep, to), device_id_type=MESH)
    for load in loads[1:]:
        load.start()
    loads[0].wait()

    lane = lax.broadcasted_iota(jnp.int32, (16, 128), 1)
    sub = lax.broadcasted_iota(jnp.int32, (16, 128), 0)
    row = lax.broadcasted_iota(jnp.int32, (128, 16), 0)
    named = jnp.zeros((128, 16), F32)
    weight = jnp.zeros((128, 16), F32)
    for k in range(4):
        hit = routes[k : k + 1, :] == row // 2
        named = named + jnp.where(hit, 1.0, 0.0)
        weight = weight + jnp.where(hit, gates[k : k + 1, :], 0.0)
    earlier = jnp.where(
        lax.broadcasted_iota(jnp.int32, (16, 16), 0) < lax.broadcasted_iota(jnp.int32, (16, 16), 1), 1.0, 0.0
    )
    slot = dot(named.astype(BF), earlier.astype(BF))
    chosen = (named > 0.5) & (jnp.abs(slot - (row % 2).astype(F32)) < 0.5)
    select = jnp.where(chosen, 1.0, 0.0)
    weight = jnp.where(chosen, weight, 0.0).T
    w_hi = weight.astype(BF)
    rest = weight - w_hi.astype(F32)
    w_mid = rest.astype(BF)
    w_lo = (rest - w_mid.astype(F32)).astype(BF)
    own = tok[...]
    rows[...] = dot(select.astype(BF), own)
    for b in range(NEP):
        asend[b] = rows[4 * b : 4 * b + 4, :].astype(BF)
    arecv[me_ep] = asend[me_ep]

    for load in loads[1:]:
        load.wait()
    for k in range(8):
        for s, source in enumerate((eg, eu)):
            for e in range(2):
                at = 128 * (2 * s + e)
                turned = source[e, :, 128 * k : 128 * k + 128].T
                for part in range(8):
                    to = 64 * (part % 2) + 16 * (part // 2)
                    wt[k, to : to + 16, at : at + 128] = turned[16 * part : 16 * part + 16, :]
        for half, source in enumerate((sg, su)):
            swt[128 * half : 128 * half + 128, 128 * k : 128 * k + 128] = source[:, 128 * k : 128 * k + 128].T
    for e in range(2):
        for half in range(2):
            for k in range(4):
                units = [ed[e, 32 * p + 16 * half : 32 * p + 16 * half + 16, :] for p in range(8 * k, 8 * k + 8)]
                at = 128 * (2 * half + e)
                dt[at : at + 128, 128 * k : 128 * k + 128] = jnp.concatenate(units, axis=0).T
    gain = pg[...].astype(F32)
    own32 = own.astype(F32)
    sxbd[...] = jnp.zeros_like(sxbd)
    xsm[...] = jnp.zeros_like(xsm)
    xbd[...] = jnp.zeros_like(xbd)
    own_gained = (own32 * gain).astype(BF)
    for g in range(8):
        sxbd[16 * g : 16 * g + 16, 128 * g : 128 * g + 128] = own_gained
    shared_part = dot(swt[...], sxbd[...], NT)
    own_squares = jnp.sum(own32 * own32, axis=1, keepdims=True)
    own_line = jnp.sum(jnp.where(lane % 16 == sub, own_squares, 0.0), axis=0, keepdims=True)
    own_line_hi = own_line.astype(BF).astype(F32)
    own_sums = jnp.where(sub == 8, own_line_hi, 0.0) + jnp.where(sub == 9, own_line - own_line_hi, 0.0)
    for p in range(NTP):
        rows[0:4, :] = shared_part[4 * p : 4 * p + 4, :]
        rows[4:8, :] = shared_part[128 + 4 * p : 132 + 4 * p, :]
        rows[8:16, :] = own_sums[8:16, :]
        ssend[p] = rows[0:16, :].astype(BF)
    srecv[me_tp] = ssend[me_tp]

    pl.semaphore_wait(barrier, 62)
    for to in far_ep:
        send(asend.at[to], arecv.at[me_ep], a_s, a_r.at[z // 4], ep=to).start()
    for to in far_tp:
        send(ssend.at[to], srecv.at[me_tp], s_s, s_r, tp=to).start()

    def rows_came(quarter):
        @pl.when(z // 4 == quarter)
        def _():
            wait_bytes(arecv.at[pl.ds(0, 7)], a_r.at[quarter])

        @pl.when(z // 4 != quarter)
        def _():
            wait_bytes(arecv.at[pl.ds(0, 8)], a_r.at[quarter])

    def rows_split(ch, start, blocks):
        count = 4 * blocks
        for b in range(blocks):
            rows[4 * b : 4 * b + 4, :] = arecv[start + b].astype(F32)
        came = rows[0:count, :]
        r0 = lax.broadcasted_iota(jnp.int32, (count, 128), 0)
        r1 = lax.broadcasted_iota(jnp.int32, (count, 128), 1)
        squares = jnp.sum(came * came, axis=1, keepdims=True)
        line = jnp.sum(jnp.where(r1 % count == r0, squares, 0.0), axis=0, keepdims=True)
        qsend[ch] = line
        qrecv[32 * ch + me_tp] = line
        gained = came * gain
        first = (r0 // 2) % 2 == 0
        return jnp.where(first, gained, 0.0).astype(BF), jnp.where(first, 0.0, gained).astype(BF)

    def squares_told(ch):
        for to in far_tp:
            send(qsend.at[ch], qrecv.at[32 * ch + me_tp], q_s, q_r.at[ch], tp=to).start()

    def small_multiplied(ch):
        e0, e1 = rows_split(ch, 8 * ch, 8)
        for half in range(2):
            for s in range(2):
                at = 64 * half + 32 * s
                xsm[ch, half, at : at + 32, 256 * s : 256 * s + 128] = e0
                xsm[ch, half, at : at + 32, 256 * s + 128 : 256 * s + 256] = e1
        for some in STAGES:
            low = jnp.concatenate([wt[ys[dy], 0:64, :] for dy in some], axis=0)
            high = jnp.concatenate([wt[ys[dy], 64:128, :] for dy in some], axis=0)
            part = dot(low, xsm[ch, 0], NT) + dot(high, xsm[ch, 1], NT)
            for k, dy in enumerate(some):
                for xp in range(NX):
                    at = 64 * k + 16 * xp
                    bsend[32 * ch + ys[dy] * NX + xp] = part[at : at + 16, :].astype(BF)
            for dy in some:
                for dx in FAR_X:
                    if dy or dx:
                        to = ys[dy] * NX + xs[dx]
                        send(bsend.at[32 * ch + to], brecv.at[32 * ch + me_tp], b_s, b_r.at[ch], tp=to).start()
        brecv[32 * ch + me_tp] = bsend[32 * ch + me_tp]
        squares_told(ch)

    def scale_of(ch):
        wait_bytes(qrecv.at[pl.ds(0, 31)], q_r.at[ch])
        return lax.rsqrt(jnp.sum(qrecv[32 * ch : 32 * ch + 32], axis=0) / D + EPS)

    def units_told(ch, units):
        hid[32 * ch + me_tp] = units.astype(BF)
        for to in far_tp:
            send(hid.at[32 * ch + me_tp], hid.at[32 * ch + me_tp], c_s, c_r.at[ch], tp=to).start()

    def small_summed(ch):
        wait_bytes(brecv.at[pl.ds(0, 31)], b_r.at[ch])
        total = jnp.sum(brecv[32 * ch : 32 * ch + 32].astype(F32), axis=0)
        v = total * scale_of(ch)
        units_told(ch, silu(v) * pltpu.roll(v, 96, 1))

    def large_multiplied():
        e0, e1 = rows_split(2, 16, 16)
        for s in range(2):
            xbd[64 * s : 64 * s + 64, 256 * s : 256 * s + 128] = e0
            xbd[64 * s : 64 * s + 64, 256 * s + 128 : 256 * s + 256] = e1
        for some in (FAR_Y[:4], FAR_Y[4:]):
            part = dot(jnp.concatenate([wt[ys[dy]] for dy in some], axis=0), xbd[...], NT)
            for k, dy in enumerate(some):
                for xp in range(NX):
                    at = 128 * k + 16 * xp
                    xsend[ys[dy] * NX + xp, 0:16, :] = part[at : at + 16, :].astype(BF)
                    xsend[ys[dy] * NX + xp, 16:32, :] = part[at + 64 : at + 80, :].astype(BF)
            for dy in some:
                yp = ys[dy]
                for dx in (2, 1, 3):
                    xp = xs[dx]
                    send(
                        xsend.at[yp * NX + xp], xrecv.at[yp * NX + x], bx_s, bx_r.at[FAR_Y.index(dy) // 4], tp=y * NX + xp
                    ).start()
        squares_told(2)

    def large_summed_over_x():
        total = None
        for at, dy in enumerate(FAR_Y):
            yp = ys[dy]
            if at % 4 == 0:
                wait_bytes(xrecv.at[pl.ds(0, 12)], bx_r.at[at // 4])
            acc = xsend[yp * NX + x].astype(F32)
            for dx in (1, 3, 2):
                acc = acc + xrecv[yp * NX + xs[dx]].astype(F32)
            if dy == 0:
                total = acc
            else:
                ysend[yp] = acc.astype(BF)
                send(ysend.at[yp], yrecv.at[y], by_s, by_r, tp=yp * NX + x).start()
        return total

    def large_summed_over_y(total):
        wait_bytes(yrecv.at[pl.ds(0, 7)], by_r)
        for dy in NEAR_Y[1:]:
            total = total + yrecv[ys[dy]].astype(F32)
        v = total * scale_of(2)
        h = silu(v) * pltpu.roll(v, 64, 1)
        units_told(2, jnp.where(lane < 64, h[0:16, :], pltpu.roll(h[16:32, :], 64, 1)))

    def given_back(ch, start, blocks):
        wait_bytes(hid.at[pl.ds(0, 31)], c_r.at[ch])
        both = dot(dt[...], hid[32 * ch : 32 * ch + 32].reshape(512, 128))
        even = (lax.broadcasted_iota(jnp.int32, (128, 128), 1) // 2) % 2 == 0
        low = jnp.where(even, both[0:128, :], both[128:256, :])
        high = jnp.where(even, both[256:384, :], both[384:512, :])
        rows[...] = (low + pltpu.roll(high, 64, 1)).T
        for b in range(blocks):
            dsend[start + b] = rows[4 * b : 4 * b + 4, :].astype(BF)
        for b in range(start, start + blocks):
            @pl.when(me_ep != b)
            def _():
                send(dsend.at[b], drecv.at[me_ep], d_s, d_r, ep=b).start()

    rows_came(0)
    small_multiplied(0)
    rows_came(2)
    rows_came(3)
    large_multiplied()
    rows_came(1)
    small_multiplied(1)
    small_summed(0)

    wait_bytes(srecv.at[pl.ds(0, 31)], s_r)
    shared_sum = jnp.sum(srecv[...].astype(F32), axis=0)
    own_scale = lax.rsqrt((shared_sum[8:9, :] + shared_sum[9:10, :]) / D + EPS)
    hsh[me_tp] = (silu(shared_sum[0:4, :] * own_scale) * (shared_sum[4:8, :] * own_scale)).astype(BF)
    for to in far_tp:
        send(hsh.at[me_tp], hsh.at[me_tp], h_s, h_r, tp=to).start()

    total2 = large_summed_over_x()
    small_summed(1)
    given_back(0, 0, 8)
    large_summed_over_y(total2)
    given_back(1, 8, 8)

    @pl.when(z // 8 == 0)
    def _():
        drecv[me_ep] = dsend[me_ep]

    @pl.when(z // 8 == 1)
    def _():
        given_back(2, 16, 16)
        drecv[me_ep] = dsend[me_ep]

    wait_bytes(hsh.at[pl.ds(0, 31)], h_r)
    for p in range(NTP):
        rows[4 * p : 4 * p + 4, :] = hsh[p].astype(F32)
    turned = rows[...].T.astype(BF)
    shared_out = jnp.zeros((16, 128), F32)
    for g in range(8):
        shared_out = shared_out + dot(turned[16 * g : 16 * g + 16, :], sd[128 * g : 128 * g + 128, :])

    wait_bytes(drecv.at[pl.ds(0, 31)], d_r)
    for b in range(NEP):
        rows[4 * b : 4 * b + 4, :] = drecv[b].astype(F32)
    given = rows[...].astype(BF)
    combined = dot(w_hi, given) + dot(w_mid, given) + dot(w_lo, given) + shared_out
    out_squares = jnp.sum(combined * combined, axis=1, keepdims=True)
    out_line = jnp.sum(jnp.where(lane == sub, out_squares, 0.0), axis=0, keepdims=True)
    esend[...] = out_line
    for to in far_tp:
        send(esend, erecv.at[me_tp], e_s, e_r, tp=to).start()
    erecv[me_tp] = out_line

    @pl.when(z // 8 == 0)
    def _():
        given_back(2, 16, 16)

    wait_bytes(erecv.at[pl.ds(0, 31)], e_r)
    all_squares = jnp.sum(erecv[...], axis=0)
    column = jnp.sum(jnp.where(lane == sub, all_squares, 0.0), axis=1, keepdims=True)
    out_scale = lax.rsqrt(column / D + EPS)
    out_ref[...] = (combined * out_scale * og[...].astype(F32)).astype(BF)

    for ref, sem in (
        (asend.at[pl.ds(0, 31)], a_s), (ssend.at[pl.ds(0, 31)], s_s), (hsh.at[pl.ds(0, 31)], h_s),
        (dsend.at[pl.ds(0, 31)], d_s), (erecv.at[pl.ds(0, 31)], e_s), (bsend.at[pl.ds(0, 62)], b_s),
        (xsend.at[pl.ds(0, 24)], bx_s), (ysend.at[pl.ds(0, 7)], by_s), (hid.at[pl.ds(0, 93)], c_s),
        (qrecv.at[pl.ds(0, 93)], q_s),
    ):
        wait_bytes(ref, sem)


def solution(mesh):
    def on_device(tokens, routes, gates, pre_gain, eg, eu, ed, sg, su, sd, out_gain):
        dma = pltpu.SemaphoreType.DMA
        hbm = pl.BlockSpec(memory_space=pl.ANY)
        vmem = pl.BlockSpec(memory_space=pltpu.VMEM)
        return pl.pallas_call(
            kernel,
            name="experts",
            out_shape=jax.ShapeDtypeStruct((16, 128), BF),
            in_specs=[hbm] + [vmem] * 3 + [hbm] * 6 + [vmem],
            out_specs=pl.BlockSpec(memory_space=pltpu.VMEM),
            scratch_shapes=[
                pltpu.VMEM((16, 128), BF), pltpu.VMEM((2, 128, 1024), BF), pltpu.VMEM((2, 128, 1024), BF),
                pltpu.VMEM((2, 1024, 128), BF), pltpu.VMEM((128, 1024), BF), pltpu.VMEM((128, 1024), BF),
                pltpu.VMEM((1024, 128), BF),
                pltpu.VMEM((8, 128, 512), BF), pltpu.VMEM((256, 1024), BF), pltpu.VMEM((512, 512), BF),
                pltpu.VMEM((32, 4, 128), BF), pltpu.VMEM((32, 4, 128), BF), pltpu.VMEM((128, 128), F32),
                pltpu.VMEM((2, 2, 128, 512), BF), pltpu.VMEM((128, 512), BF), pltpu.VMEM((128, 1024), BF),
                pltpu.VMEM((32, 16, 128), BF), pltpu.VMEM((32, 16, 128), BF), pltpu.VMEM((32, 4, 128), BF),
                pltpu.VMEM((64, 16, 128), BF), pltpu.VMEM((64, 16, 128), BF),
                pltpu.VMEM((32, 32, 128), BF), pltpu.VMEM((32, 32, 128), BF),
                pltpu.VMEM((8, 32, 128), BF), pltpu.VMEM((8, 32, 128), BF),
                pltpu.VMEM((3, 1, 128), F32), pltpu.VMEM((96, 1, 128), F32),
                pltpu.VMEM((96, 16, 128), BF),
                pltpu.VMEM((32, 4, 128), BF), pltpu.VMEM((32, 4, 128), BF),
                pltpu.VMEM((1, 128), F32), pltpu.VMEM((32, 1, 128), F32),
                dma((7,)), dma, dma((4,)), dma, dma, dma, dma, dma, dma((2,)), dma, dma((2,)), dma, dma,
                dma, dma((3,)), dma, dma((3,)), dma, dma, dma, dma,
            ],
            compiler_params=pltpu.CompilerParams(collective_id=0, has_side_effects=True, vmem_limit_bytes=55212 * 1024),
        )(tokens, routes.T, gates.T, pre_gain.reshape(1, 128), eg, eu, ed, sg, su, sd, out_gain.reshape(1, 128))

    return jax.shard_map(
        on_device,
        mesh=mesh,
        in_specs=(
            P("ep", "tp"), P("ep", None), P("ep", None), P("tp"), P("ep", "tp", None), P("ep", "tp", None),
            P("ep", None, "tp"), P("tp", None), P("tp", None), P(None, "tp"), P("tp"),
        ),
        out_specs=P("ep", "tp"),
        check_vma=False,
    )
```

time: 61.9 us -> 60.5 us (0.977)
  Pallas kernels: 60.1 us -> 59 us
    pallas_call x1, Pallas kernels: 60.1 us -> 59 us  [on_device(): pl.pallas_call(kernel, name='experts', out_shape=jax.ShapeDtypeStruct((16...]
    unnamed x1 -> x9, local copies, waits for them, and re-layouts: 1.28 us -> 1.28 us
where the time goes in v3:
time: 60.5 us; the launch traced here: 60.3 us
  Pallas kernels  59 us (98%)
  local copies, waits for them, and re-layouts  1.28 us (2%)
    pallas_call x1, Pallas kernels, on_device(): pl.pallas_call(kernel, name='experts', out_shape=jax.ShapeDtypeStruct((16...  59 us
    unnamed x9, local copies, waits for them, and re-layouts  1.28 us

profile of v3, /device:TPU:1, one launch (start us, length us, event | category | flops | bytes accessed | tf_op | source)
XLA Modules:
  0.0 60.3 jit_solution(3281418144889031271)
XLA Ops:
  0.0 0.0 copy-start.1
  0.0 0.0 copy-start
  0.0 0.0 copy-start.2
  0.0 0.0 copy-start.3
  0.0 0.7 %copy-done.1 = f32[16,4]{0,1:T(4,128)S(1)} copy-done((f32[16,4]{0,1:T(4,128)S(1)}, f32[16,4]{0,1:T(4,128)}, u32[]{:S(2)}) %copy-start.1) | copy-done | bytes 280
  0.7 0.0 copy-done
  0.7 0.0 copy-done.2
  0.7 0.0 copy-done.3
  0.7 59.0 %experts.1 = bf16[16,128]{1,0:T(8,128)(2,1)S(1)} custom-call(bf16[16,128]{1,0:T(8,128)(2,1)} %tok_h.1, s32[4,16]{1,0:T(4,128)S(1)} %bitcast.4, f32[4,16]{1,0:T(4,128)S(1)} %bitcast.5, bf16[1,128]{1,0:T(2,128)(2,1)S(1)} %bitcast.6, bf16[2,128,1024]{2,1,0:T(8,128)(2,1)} %eg_h.1, bf16[2,128,1024]{2,1,0:T(8,128)(2,1)} %eu_h.1, bf16[2,1024,128]{2,1,0:T(8,128)(2,1)} %ed_h.1, ...), custom_call_target="tpu_custom_call" | custom-call | tf_op jit(solution)/shard_map/experts/pallas_call | solution.py:342
  59.7 0.6 copy.13
Async XLA Ops:
  0.0 0.7 %copy-start.1 = (f32[16,4]{0,1:T(4,128)S(1)}, f32[16,4]{0,1:T(4,128)}, u32[]{:S(2)}) copy-start(f32[16,4]{0,1:T(4,128)} %param.13) | copy-start | bytes 772
  0.0 0.7 %copy-start = (s32[16,4]{0,1:T(4,128)S(1)}, s32[16,4]{0,1:T(4,128)}, u32[]{:S(2)}) copy-start(s32[16,4]{0,1:T(4,128)} %param.12) | copy-start | bytes 772
  0.0 0.7 %copy-start.2 = (bf16[128]{0:T(256)(128)(2,1)S(1)}, bf16[128]{0:T(256)(128)(2,1)}, u32[]{:S(2)}) copy-start(bf16[128]{0:T(256)(128)(2,1)} %param.14) | copy-start | bytes 772
  0.0 0.7 %copy-start.3 = (bf16[128]{0:T(256)(128)(2,1)S(1)}, bf16[128]{0:T(256)(128)(2,1)}, u32[]{:S(2)}) copy-start(bf16[128]{0:T(256)(128)(2,1)} %param.21) | copy-start | bytes 772

commit v4 on v3

--- a/solution.py
+++ b/solution.py
@@ -16,7 +16,7 @@
 FAR_Y = (4, 3, 5, 2, 6, 1, 7, 0)
 NEAR_Y = (0, 1, 7, 2, 6, 3, 5, 4)
 FAR_X = (2, 1, 3, 0)
-STAGES = ((4, 3, 5), (2, 6, 1, 7, 0))
+STAGES = ((4,), (3, 5), (2, 6, 1, 7, 0))
 NT = (((1,), (1,)), ((), ()))
 NN = (((1,), (0,)), ((), ()))
 
@@ -169,6 +169,7 @@
 
     def small_multiplied(ch):
         e0, e1 = rows_split(ch, 8 * ch, 8)
+        squares_told(ch)
         for half in range(2):
             for s in range(2):
                 at = 64 * half + 32 * s
@@ -188,7 +189,6 @@
                         to = ys[dy] * NX + xs[dx]
                         send(bsend.at[32 * ch + to], brecv.at[32 * ch + me_tp], b_s, b_r.at[ch], tp=to).start()
         brecv[32 * ch + me_tp] = bsend[32 * ch + me_tp]
-        squares_told(ch)
 
     def scale_of(ch):
         wait_bytes(qrecv.at[pl.ds(0, 31)], q_r.at[ch])
@@ -307,7 +307,8 @@
     for b in range(NEP):
         rows[4 * b : 4 * b + 4, :] = drecv[b].astype(F32)
     given = rows[...].astype(BF)
-    combined = dot(w_hi, given) + dot(w_mid, given) + dot(w_lo, given) + shared_out
+    parts = dot(jnp.concatenate([w_hi, w_mid, w_lo], axis=0), given)
+    combined = parts[0:16, :] + parts[16:32, :] + parts[32:48, :] + shared_out
     out_squares = jnp.sum(combined * combined, axis=1, keepdims=True)
     out_line = jnp.sum(jnp.where(lane == sub, out_squares, 0.0), axis=0, keepdims=True)
     esend[...] = out_line

time: 60.5 us -> 59.3 us (0.980)
  Pallas kernels: 59 us -> 57.8 us
    pallas_call x1, Pallas kernels: 59 us -> 57.8 us  [on_device(): pl.pallas_call(kernel, name='experts', out_shape=jax.ShapeDtypeStruct((16...]
where the time goes in v4:
time: 59.3 us; the launch traced here: 59.1 us
  Pallas kernels  57.8 us (97%)
  local copies, waits for them, and re-layouts  1.28 us (2%)
    pallas_call x1, Pallas kernels, on_device(): pl.pallas_call(kernel, name='experts', out_shape=jax.ShapeDtypeStruct((16...  57.8 us
    unnamed x9, local copies, waits for them, and re-layouts  1.28 us

profile of v4, /device:TPU:1, one launch (start us, length us, event | category | flops | bytes accessed | tf_op | source)
XLA Modules:
  0.0 59.1 jit_solution(8394120215195411951)
XLA Ops:
  0.0 0.0 copy-start.1
  0.0 0.0 copy-start
  0.0 0.0 copy-start.2
  0.0 0.0 copy-start.3
  0.0 0.7 %copy-done.1 = f32[16,4]{0,1:T(4,128)S(1)} copy-done((f32[16,4]{0,1:T(4,128)S(1)}, f32[16,4]{0,1:T(4,128)}, u32[]{:S(2)}) %copy-start.1) | copy-done | bytes 280
  0.7 0.0 copy-done
  0.7 0.0 copy-done.2
  0.7 0.0 copy-done.3
  0.7 57.8 %experts.1 = bf16[16,128]{1,0:T(8,128)(2,1)S(1)} custom-call(bf16[16,128]{1,0:T(8,128)(2,1)} %tok_h.1, s32[4,16]{1,0:T(4,128)S(1)} %bitcast.4, f32[4,16]{1,0:T(4,128)S(1)} %bitcast.5, bf16[1,128]{1,0:T(2,128)(2,1)S(1)} %bitcast.6, bf16[2,128,1024]{2,1,0:T(8,128)(2,1)} %eg_h.1, bf16[2,128,1024]{2,1,0:T(8,128)(2,1)} %eu_h.1, bf16[2,1024,128]{2,1,0:T(8,128)(2,1)} %ed_h.1, ...), custom_call_target="tpu_custom_call" | custom-call | tf_op jit(solution)/shard_map/experts/pallas_call | solution.py:343
  58.5 0.6 %copy.13 = bf16[16,128]{1,0:T(8,128)(2,1)} copy(bf16[16,128]{1,0:T(8,128)(2,1)S(1)} %experts.1) | data formatting | bytes 8192
Async XLA Ops:
  0.0 0.7 %copy-start.1 = (f32[16,4]{0,1:T(4,128)S(1)}, f32[16,4]{0,1:T(4,128)}, u32[]{:S(2)}) copy-start(f32[16,4]{0,1:T(4,128)} %param.13) | copy-start | bytes 772
  0.0 0.7 %copy-start = (s32[16,4]{0,1:T(4,128)S(1)}, s32[16,4]{0,1:T(4,128)}, u32[]{:S(2)}) copy-start(s32[16,4]{0,1:T(4,128)} %param.12) | copy-start | bytes 772
  0.0 0.7 %copy-start.2 = (bf16[128]{0:T(256)(128)(2,1)S(1)}, bf16[128]{0:T(256)(128)(2,1)}, u32[]{:S(2)}) copy-start(bf16[128]{0:T(256)(128)(2,1)} %param.14) | copy-start | bytes 772
  0.0 0.7 %copy-start.3 = (bf16[128]{0:T(256)(128)(2,1)S(1)}, bf16[128]{0:T(256)(128)(2,1)}, u32[]{:S(2)}) copy-start(bf16[128]{0:T(256)(128)(2,1)} %param.21) | copy-start | bytes 772
